TPU v7x, 32 devices: a whole 2x2x4 slice. The times are simulated.
32 devices in a mesh: sp: 8 (over z, y), tp: 4 (over x, core).
Axes of the slice: x: 2, y: 2, z: 4, core: 2. Of those that a mesh axis runs over, the one named last changes fastest.
Arguments:
- queries: bfloat16 [8192, 1024], P('sp', 'tp'), may hold values from -6 to 6
- keys: bfloat16 [8192, 1024], P('sp', 'tp'), may hold values from -6 to 6
- values: bfloat16 [8192, 1024], P('sp', 'tp'), may hold values from -6 to 6
- gates: bfloat16 [8192, 1024], P('sp', 'tp'), may hold values from -6 to 6
- log_decay: float32 [8192, 8], P('sp', 'tp'), may hold values from -1.6 to 0, as said below
- norm_gain: float32 [8, 128], P('tp'), may hold values from 0.1 to 1.9
- out_weight: bfloat16 [1024, 2048], P('tp'), may hold values from -0.1875 to 0.1875
- resid: bfloat16 [8192, 2048], P(('sp', 'tp')), may hold values from -6 to 6
- post_mix_gain: float32 [2048], replicated, may hold values from 0.1 to 1.9
- pre_ffn_gain: float32 [2048], replicated, may hold values from 0.1 to 1.9
- w_gate: bfloat16 [2048, 5632], P('sp', 'tp'), may hold values from -0.125 to 0.125
- w_up: bfloat16 [2048, 5632], P('sp', 'tp'), may hold values from -0.125 to 0.125
- w_down: bfloat16 [5632, 2048], P('tp', 'sp'), may hold values from -0.078125 to 0.078125
- post_ffn_gain: float32 [2048], replicated, may hold values from 0.1 to 1.9
Outputs:
- updated: bfloat16 [8192, 2048], P(('sp', 'tp'))
Inputs may be any that keep to these rules, and one draw needn't show every extreme that they name: `log_decay`: every entry is negative.
All inputs are finite; a program needn't handle non-finite values.
Results may differ from a plain program's by a relative error of at most 0.02.
Values may be sent and summed in bfloat16 or wider, within the bound.
A program may use at most 128 MiB of HBM per device.

v0:
```python
import jax
import jax.numpy as jnp
from jax import lax
from jax.sharding import PartitionSpec as P

BLOCK = 512
EPSILON = 1e-06


def entering(x, axis, join, neutral):
    place = lax.axis_index(axis)
    gathered = jax.tree.map(
        lambda a, kind: lax.all_gather(a.astype(kind), axis), x, (jnp.bfloat16, jnp.bfloat16)
    )
    state = jax.tree.map(lambda a, e: jnp.zeros_like(a) + jnp.asarray(e, a.dtype), x, neutral)

    def one(step, state):
        return join(
            state,
            jax.tree.map(
                lambda a, own: lax.dynamic_index_in_dim(a, step, 0, False).astype(own.dtype),
                gathered,
                x,
            ),
        )

    return lax.fori_loop(0, place, one, state)


def rms_norm(values_in, gain_vec):
    widened = values_in.astype(jnp.float32)
    return (
        widened
        * lax.rsqrt(jnp.mean(widened * widened, axis=-1, keepdims=True) + EPSILON)
        * gain_vec
    )


def block_step(carried, pieces):
    query_blk, key_blk, value_blk, decay_blk = pieces
    length = query_blk.shape[1]
    key_scale = query_blk.shape[2] ** (-0.5)
    cumulative = jnp.cumsum(decay_blk, axis=1)
    log_gap = cumulative[:, :, None] - cumulative[:, None, :]
    causal = lax.broadcasted_iota(jnp.int32, (length, length), 0) >= lax.broadcasted_iota(
        jnp.int32, (length, length), 1
    )
    weight = jnp.where(causal[None], jnp.exp(jnp.minimum(log_gap, 0.0)), 0.0)
    products = jnp.einsum("htd,hsd->hts", query_blk, key_blk, preferred_element_type=jnp.float32)
    scores = (products * key_scale * weight).astype(jnp.bfloat16)
    within = jnp.einsum("hts,hsd->htd", scores, value_blk, preferred_element_type=jnp.float32)
    carried_term = (
        jnp.einsum(
            "htd,hde->hte", query_blk.astype(jnp.float32), carried, precision=lax.Precision.HIGHEST
        )
        * jnp.exp(cumulative)[:, :, None]
    )
    to_end = jnp.exp(cumulative[:, -1:] - cumulative) * key_scale
    scaled_keys = (key_blk.astype(jnp.float32) * to_end[:, :, None]).astype(jnp.bfloat16)
    added = jnp.einsum("hsd,hse->hde", scaled_keys, value_blk, preferred_element_type=jnp.float32)
    carried = jnp.exp(cumulative[:, -1])[:, None, None] * carried + added
    return (carried, within + carried_term)


def to_blocks(matrix, block_len, head_count):
    row_count = matrix.shape[0]
    return matrix.reshape(row_count // block_len, block_len, head_count, -1).transpose(0, 2, 1, 3)


def finish_heads(retention, gates, norm_gain):
    centered = retention - jnp.mean(retention, axis=-1, keepdims=True)
    variance = jnp.mean(centered * centered, axis=-1, keepdims=True)
    normed = centered * lax.rsqrt(variance + EPSILON) * norm_gain[None]
    gate_vals = gates.astype(jnp.float32).reshape(normed.shape)
    return (jax.nn.silu(gate_vals) * normed).reshape(normed.shape[0], -1).astype(jnp.bfloat16)


def combine_states(earlier, later):
    return (earlier[0] * later[0], later[0][:, None, None] * earlier[1] + later[1])


def per_device(
    queries,
    keys,
    values,
    gates,
    log_decay,
    norm_gain,
    out_weight,
    resid,
    post_mix_gain,
    pre_ffn_gain,
    w_gate,
    w_up,
    w_down,
    post_ffn_gain,
):
    row_count = queries.shape[0]
    head_count = log_decay.shape[1]
    head_dim = queries.shape[1] // head_count
    block_count = row_count // BLOCK
    query_blocks = to_blocks(queries, BLOCK, head_count)
    key_blocks = to_blocks(keys, BLOCK, head_count)
    value_blocks = to_blocks(values, BLOCK, head_count)
    decay_blocks = log_decay.reshape(block_count, BLOCK, head_count).transpose(0, 2, 1)
    start_state = jnp.zeros((head_count, head_dim, head_dim), jnp.float32)
    local_state, outputs = lax.scan(
        block_step, start_state, (query_blocks, key_blocks, value_blocks, decay_blocks)
    )
    retention = outputs.transpose(0, 2, 1, 3).reshape(row_count, head_count, head_dim)
    cumulative = jnp.cumsum(log_decay, axis=0)
    local_decay = jnp.exp(cumulative[-1])
    identity = (jnp.ones_like(local_decay), jnp.zeros_like(local_state))
    incoming = entering((local_decay, local_state), "sp", combine_states, identity)
    query_rows = queries.reshape(row_count, head_count, head_dim).astype(jnp.float32)
    retention = (
        retention
        + jnp.einsum("thd,hde->the", query_rows, incoming[1], precision=lax.Precision.HIGHEST)
        * jnp.exp(cumulative)[:, :, None]
    )
    retained = finish_heads(retention, gates, norm_gain)
    quarter = resid.shape[0]
    regrouped = lax.all_to_all(retained, "tp", split_axis=0, concat_axis=1, tiled=True)
    group_rows = out_weight.shape[0]
    empty_mix = jnp.zeros((quarter, out_weight.shape[1]), jnp.float32)
    running = empty_mix
    shard_piece = lax.all_gather(out_weight, "tp", axis=0, tiled=True)
    for offset in range(shard_piece.shape[0] // group_rows):
        columns = lax.dynamic_slice_in_dim(regrouped, offset * group_rows, group_rows, 1)
        part = jnp.dot(
            columns,
            shard_piece[offset * group_rows : (offset + 1) * group_rows],
            preferred_element_type=jnp.float32,
        )
        running = running + part.astype(jnp.bfloat16).astype(jnp.float32)
    mixed = running
    mixed = mixed.astype(jnp.bfloat16)
    middle = (resid.astype(jnp.float32) + rms_norm(mixed, post_mix_gain)).astype(jnp.bfloat16)
    ffn_input = rms_norm(middle, pre_ffn_gain).astype(jnp.bfloat16)
    gathered = lax.all_gather(ffn_input, "tp", axis=0, tiled=True)
    columns = gathered
    gate_act = jnp.dot(
        columns,
        lax.all_gather(w_gate, "sp", axis=0, tiled=True),
        preferred_element_type=jnp.float32,
    )
    up_act = jnp.dot(
        columns, lax.all_gather(w_up, "sp", axis=0, tiled=True), preferred_element_type=jnp.float32
    )
    down_full = lax.all_gather(w_down, "sp", axis=1, tiled=True)
    hidden = (jax.nn.silu(gate_act) * up_act).astype(jnp.bfloat16)
    branch = lax.psum_scatter(
        jnp.dot(hidden, down_full, preferred_element_type=jnp.float32)
        .astype(jnp.bfloat16)
        .astype(jnp.float32)
        .astype(jnp.bfloat16),
        "tp",
        scatter_dimension=0,
        tiled=True,
    )
    return (middle.astype(jnp.float32) + rms_norm(branch, post_ffn_gain)).astype(jnp.bfloat16)


def solution(mesh):
    in_specs = (
        P("sp", "tp"),
        P("sp", "tp"),
        P("sp", "tp"),
        P("sp", "tp"),
        P("sp", "tp"),
        P("tp", None),
        P("tp", None),
        P(("sp", "tp"), None),
        P(),
        P(),
        P("sp", "tp"),
        P("sp", "tp"),
        P("tp", "sp"),
        P(),
    )
    out_specs = P(("sp", "tp"), None)
    return jax.shard_map(
        per_device, mesh=mesh, in_specs=in_specs, out_specs=out_specs, check_vma=False
    )
```

profile of v0, /device:TPU:0, one launch (start us, length us, event | category | flops | bytes accessed | tf_op | source)
XLA Modules:
  0.0 438.4 jit_solution(6785753459974340258)
XLA Ops:
  10.0 22.3 %all-gather.1 = bf16[8,1,2]{2,1,0:T(2,128)(2,1)S(1)} all-gather(bf16[1,1,2]{2,1,0:T(2,128)(2,1)S(1)} %bitcast.154), channel_id=1, replica_groups=mesh['sp'=8,'tp'=4] {'sp'}, dimensions={0}, use_global_device_ids=true | all-gather | bytes 36 | tf_op jit(solution)/shard_map/all_gather | solution.py:13
  32.8 9.6 %while.26 = (s32[]{:T(128)}, f32[2,128,128]{2,1,0:T(8,128)S(1)}, f32[2,2,512,128]{3,2,1,0:T(8,128)}, f32[2,2,512]{2,1,0:T(2,128)S(1)}, bf16[2,2,512,128]{3,1,2,0...) while((s32[]{:T(128)}, f32[2,128,128]{2,1,0:T(8,128)S(1)}, ...), condition=%wide.region_3.4_spmd.clone, body=%wide.region_0.3_spmd.clone.sunk | while | flops 507643936 | bytes 5702508 | solution.py:107
  34.5 1.0 fusion.75
  35.8 1.2 fusion.76
  39.3 1.0 fusion.75
  40.6 1.2 fusion.76
  42.4 1.6 copy.57
  44.1 0.9 reshape.175
  45.2 33.1 %all-gather = bf16[16,128,128]{2,1,0:T(8,128)(2,1)S(1)} all-gather(bf16[2,128,128]{2,1,0:T(8,128)(2,1)S(1)} %convert_element_type.103), channel_id=2, replica_groups=mesh['sp'=8,'tp'=4] {'sp'}, dimensions={0}, use_global_device_ids=true | all-gather | bytes 589824 | tf_op jit(solution)/shard_map/all_gather | solution.py:13
  78.4 0.7 fusion.51
  80.1 11.4 %all_to_all.16 = bf16[4,256,256]{1,2,0:T(8,128)(2,1)S(1)} all-to-all(bf16[4,256,256]{1,2,0:T(8,128)(2,1)S(1)} %copy.62), channel_id=1, replica_groups=mesh['sp'=8,'tp'=4] {'tp'}, dimensions={0} | all-to-all | bytes 1048576 | tf_op jit(solution)/shard_map/all_to_all | solution.py:123
  91.5 1.8 fusion.22
  93.4 1.7 fusion.23
  95.6 0.8 fusion.25
  97.4 1.3 fusion.33
  100.1 41.9 %all-gather.12.cloned.1.call-done = bf16[2048,1408]{1,0:T(8,128)(2,1)} async-done(((bf16[256,1408]{1,0:T(8,128)(2,1)}), bf16[2048,1408]{1,0:T(8,128)(2,1)}) %all-gather.12.cloned.1.call-update) | async-done | bytes 5767184 | tf_op jit(solution)/shard_map/all_gather | solution.py:144
  142.0 34.2 %all-gather.10.cloned.1.call-done = bf16[1024,2048]{1,0:T(8,128)(2,1)} async-done(((bf16[256,2048]{1,0:T(8,128)(2,1)}), bf16[1024,2048]{1,0:T(8,128)(2,1)}) %all-gather.10.cloned.1.call-update) | async-done | bytes 4194320 | tf_op jit(solution)/shard_map/all_gather | solution.py:140
  176.3 11.7 %fusion.52 = f32[1024,1408]{1,0:T(8,128)} fusion(bf16[1024,2048]{1,0:T(8,128)(2,1)} %all-gather.10.cloned.1.call-done, bf16[2048,1408]{1,0:T(8,128)(2,1)} %all-gather.12.cloned.1.call-done), kind=kOutput, calls=%fused_computation.97 | convolution fusion | flops 5905580032 | bytes 15728640 | tf_op jit(solution)/shard_map/dot_general | solution.py:142
  188.0 82.7 %all-gather.14.cloned.1.call-done = bf16[2048,1408]{1,0:T(8,128)(2,1)} async-done(((bf16[256,1408]{1,0:T(8,128)(2,1)}), bf16[2048,1408]{1,0:T(8,128)(2,1)}) %all-gather.14.cloned.1.call-update) | async-done | bytes 5767184 | tf_op jit(solution)/shard_map/all_gather | solution.py:148
  270.7 93.2 %all-gather.16.cloned.1.call-done = bf16[1408,2048]{1,0:T(8,128)(2,1)} async-done(((bf16[1408,256]{1,0:T(8,128)(2,1)}), bf16[1408,2048]{1,0:T(8,128)(2,1)}) %all-gather.16.cloned.1.call-update) | async-done | bytes 5767184 | tf_op jit(solution)/shard_map/all_gather | solution.py:150
  363.9 20.5 %convolution_convert_fusion = bf16[1024,2048]{1,0:T(8,128)(2,1)} fusion(bf16[1408,2048]{1,0:T(8,128)(2,1)} %all-gather.16.cloned.1.call-done, f32[1024,1408]{1,0:T(8,128)} %fusion.52, bf16[1024,2048]{1,0:T(8,128)(2,1)} %all-gather.10.cloned.1.call-done, bf16[2048,1408]{1,0:T(8,128)(2,1)} %all-gather.14.cloned.1.call-done), kind=kOutput, calls=%fused_computation.38 | convolution fusion | flops 11821907968 | bytes 25690112 | tf_op jit(solution)/shard_map/dot_general | solution.py:153
  384.5 42.9 %reduce-scatter.2.cloned.1.call-done = bf16[256,2048]{1,0:T(8,128)(2,1)} async-done(((bf16[1024,2048]{1,0:T(8,128)(2,1)}), bf16[256,2048]{1,0:T(8,128)(2,1)}) %reduce-scatter.2.cloned.1.call-update) | async-done | bytes 1048592 | tf_op jit(solution)/shard_map/reduce_scatter | solution.py:152
  427.4 1.5 fusion.29
  428.9 2.6 fusion.34
  (96 shorter events, 13.0 us)
Async XLA Ops:
  6.5 25.8 %copy-start.5 = (bf16[1024,256]{1,0:T(8,128)(2,1)S(1)}, bf16[1024,256]{1,0:T(8,128)(2,1)}, u32[]{:S(2)}) copy-start(bf16[1024,256]{1,0:T(8,128)(2,1)} %param.19) | copy-start | bytes 1572868
  6.5 26.0 %copy-start.6 = (bf16[1024,256]{1,0:T(8,128)(2,1)S(1)}, bf16[1024,256]{1,0:T(8,128)(2,1)}, u32[]{:S(2)}) copy-start(bf16[1024,256]{1,0:T(8,128)(2,1)} %param.20) | copy-start | bytes 1572868
  6.5 26.1 %copy-start.1 = (bf16[1024,256]{1,0:T(8,128)(2,1)S(1)}, bf16[1024,256]{1,0:T(8,128)(2,1)}, u32[]{:S(2)}) copy-start(bf16[1024,256]{1,0:T(8,128)(2,1)} %param.18) | copy-start | bytes 1572868
  6.5 85.0 %all-gather.8.cloned.1.call-start = ((), (), s32[]{:S(2)}) async-start(), calls=%async_computation.2 | async-start | bytes 5242880 | tf_op jit(solution)/shard_map/all_gather | solution.py:127
  7.3 25.5 %copy-start.7 = (f32[1024,2]{0,1:T(2,128)S(1)}, f32[1024,2]{0,1:T(2,128)}, u32[]{:S(2)}) copy-start(f32[1024,2]{0,1:T(2,128)} %param.22) | copy-start | bytes 24580
  7.3 134.8 %all-gather.12.cloned.1.call-start = ((), (), s32[]{:S(2)}) async-start(), calls=%async_computation.4 | async-start | bytes 6488064 | tf_op jit(solution)/shard_map/all_gather | solution.py:144
  8.0 168.3 %all-gather.10.cloned.1.call-start = ((), (), s32[]{:S(2)}) async-start(), calls=%async_computation.3 | async-start | bytes 5242880 | tf_op jit(solution)/shard_map/all_gather | solution.py:140
  42.4 2.6 copy-start.4
  45.0 33.4 %copy-start.2 = (bf16[1024,256]{1,0:T(8,128)(2,1)S(1)}, bf16[1024,256]{1,0:T(8,128)(2,1)}, u32[]{:S(2)}) copy-start(bf16[1024,256]{1,0:T(8,128)(2,1)} %param.18) | copy-start | bytes 1572868
  78.3 0.9 copy-start.11
  91.5 3.5 copy-start
  95.5 1.2 copy-start.3
  95.5 1.2 copy-start.8
  96.4 1.1 copy-start.9
  98.7 171.9 %all-gather.14.cloned.1.call-start = ((), (), s32[]{:S(2)}) async-start(), calls=%async_computation.5 | async-start | bytes 6488064 | tf_op jit(solution)/shard_map/all_gather | solution.py:148
  99.3 264.6 %all-gather.16.cloned.1.call-start = ((), (), s32[]{:S(2)}) async-start(), calls=%async_computation.6 | async-start | bytes 6488064 | tf_op jit(solution)/shard_map/all_gather | solution.py:150
  99.9 327.5 %reduce-scatter.2.cloned.1.call-start = ((), (), s32[]{:S(2)}) async-start(), calls=%async_computation.7 | async-start | bytes 5242880 | tf_op jit(solution)/shard_map/reduce_scatter | solution.py:152
  384.4 44.5 %copy-start.10 = (f32[2048]{0:T(1024)S(1)}, f32[2048]{0:T(1024)}, u32[]{:S(2)}) copy-start(f32[2048]{0:T(1024)} %param.31) | copy-start | bytes 24580
Sparse Core Ops, SparseCore 0:
  8.9 37.1 all-gather.7
  48.3 93.7 all-gather.11
  143.6 32.6 all-gather.9
  178.3 92.3 all-gather.13
  272.6 91.2 all-gather.15
  384.6 42.7 reduce-scatter.1
where the time goes:
time: 439 us; the launch traced here: 438 us
  waiting for transfers between devices  297 us (68%)
  blocking collectives  66.8 us (15%)
  matrix products  43.3 us (10%)
  between operations  13.8 us (3%)
  other arithmetic  9.76 us (2%)
  local copies, waits for them, and re-layouts  6.82 us (2%)
    all_gather x1, waiting for transfers between devices, per_device(): down_full = lax.all_gather(w_down, 'sp', axis=1, tiled=True)  93.2 us
    all_gather x1, waiting for transfers between devices, per_device(): lax.all_gather(w_up, 'sp', axis=0, tiled=True)  82.7 us
    all_gather x2, blocking collectives, entering(): lax.all_gather(a.astype(kind), axis)  55.4 us
    reduce_scatter x1, waiting for transfers between devices, per_device(): lax.psum_scatter(jnp.dot(hidden, down_full, preferred_element_type=jnp.fl...  42.9 us
    all_gather x1, waiting for transfers between devices, per_device(): lax.all_gather(w_gate, 'sp', axis=0, tiled=True)  41.9 us
    all_gather x1, waiting for transfers between devices, per_device(): gathered = lax.all_gather(ffn_input, 'tp', axis=0, tiled=True)  34.2 us
    dot_general x1, matrix products, per_device(): jnp.dot(hidden, down_full, preferred_element_type=jnp.float32)  20.5 us
    dot_general x1, matrix products, per_device(): jnp.dot(columns, lax.all_gather(w_gate, 'sp', axis=0, tiled=True), prefer...  11.7 us
  transfers between devices with their start and end apart: 6, of which 5 were waited for; matrix products, arithmetic and copies ran while one was open for 8% of the time, Pallas kernels for 0%

commit v1 on v0

--- a/solution.py
+++ b/solution.py
@@ -1,10 +1,35 @@
+import functools
 import jax
 import jax.numpy as jnp
 from jax import lax
 from jax.sharding import PartitionSpec as P
+from jax.lax import axis_index, axis_size, ppermute
 
 BLOCK = 512
 EPSILON = 1e-06
+
+
+def see_the_panel(array_in, join_dim):
+    cores_n = axis_size("sp")
+    i = 0
+    in_order = []
+    while i < cores_n:
+        in_order.append((i, (i + 1) % cores_n))
+        i += 1
+
+    def inputs_clear(all_values):
+        if len(all_values) == cores_n:
+            return all_values
+        return inputs_clear([ppermute(all_values[0], axis_name="sp", perm=in_order), *all_values])
+
+    return jnp.roll(
+        jnp.concatenate(inputs_clear([array_in]), axis=join_dim),
+        (axis_index("sp") + 1) * array_in.shape[join_dim],
+        axis=join_dim,
+    )
+
+
+indices_show = functools.partial(see_the_panel, join_dim=1)
 
 
 def entering(x, axis, join, neutral):
@@ -147,7 +172,7 @@
     up_act = jnp.dot(
         columns, lax.all_gather(w_up, "sp", axis=0, tiled=True), preferred_element_type=jnp.float32
     )
-    down_full = lax.all_gather(w_down, "sp", axis=1, tiled=True)
+    down_full = indices_show(w_down)
     hidden = (jax.nn.silu(gate_act) * up_act).astype(jnp.bfloat16)
     branch = lax.psum_scatter(
         jnp.dot(hidden, down_full, preferred_element_type=jnp.float32)

time: 439 us -> 424 us (0.966)
  waiting for transfers between devices: 297 us -> 253 us
  local copies, waits for them, and re-layouts: 6.82 us -> 36.7 us
    ppermute x0 -> x7, waiting for transfers between devices: none -> 203 us  [inputs_clear(): ppermute(all_values[0], axis_name='sp', perm=in_order)]
    all_gather x1 -> x0, waiting for transfers between devices: 93.2 us -> none  [per_device(): down_full = lax.all_gather(w_down, 'sp', axis=1, tiled=True)]
    all_gather x1, waiting for transfers between devices: 82.7 us -> 0.01 us  [per_device(): lax.all_gather(w_up, 'sp', axis=0, tiled=True)]
    all_gather x1, waiting for transfers between devices: 41.9 us -> 0.01 us  [per_device(): lax.all_gather(w_gate, 'sp', axis=0, tiled=True)]
    all_gather x1, waiting for transfers between devices: 34.2 us -> 0.01 us  [per_device(): gathered = lax.all_gather(ffn_input, 'tp', axis=0, tiled=True)]
    unnamed x26 -> x51, local copies, waits for them, and re-layouts: 1.16 us -> 24 us
    reduce_scatter x1, waiting for transfers between devices: 42.9 us -> 48.6 us  [per_device(): lax.psum_scatter(jnp.dot(hidden, down_full, preferred_element_type=jnp.fl...]
  transfers between devices with their start and end apart: 6 -> 12, of which waited for: 5 -> 8; matrix products, arithmetic and copies ran while one was open for 8% -> 15% of each run, Pallas kernels for 0% -> 0%
where the time goes in v1:
time: 424 us; the launch traced here: 423 us
  waiting for transfers between devices  253 us (60%)
  blocking collectives  67.2 us (16%)
  matrix products  43.2 us (10%)
  local copies, waits for them, and re-layouts  36.7 us (9%)
  between operations  13.4 us (3%)
  other arithmetic  9.77 us (2%)
    ppermute x7, waiting for transfers between devices, inputs_clear(): ppermute(all_values[0], axis_name='sp', perm=in_order)  203 us
    all_gather x2, blocking collectives, entering(): lax.all_gather(a.astype(kind), axis)  56 us
    reduce_scatter x1, waiting for transfers between devices, per_device(): lax.psum_scatter(jnp.dot(hidden, down_full, preferred_element_type=jnp.fl...  48.6 us
    unnamed x51, local copies, waits for them, and re-layouts  24 us
    dot_general x1, matrix products, per_device(): jnp.dot(hidden, down_full, preferred_element_type=jnp.float32)  20.6 us
    dot_general x1, matrix products, per_device(): jnp.dot(columns, lax.all_gather(w_gate, 'sp', axis=0, tiled=True), prefer...  11.7 us
    all_to_all x1, blocking collectives, per_device(): lax.all_to_all(retained, 'tp', split_axis=0, concat_axis=1, tiled=True)  11.2 us
  transfers between devices with their start and end apart: 12, of which 8 were waited for; matrix products, arithmetic and copies ran while one was open for 15% of the time, Pallas kernels for 0%

profile of v1, /device:TPU:0, one launch (start us, length us, event | category | flops | bytes accessed | tf_op | source)
XLA Modules:
  0.0 423.3 jit_solution(6351513006068582303)
XLA Ops:
  8.1 2.2 copy.53
  14.0 22.3 %all-gather.1 = bf16[8,1,2]{2,1,0:T(2,128)(2,1)S(1)} all-gather(bf16[1,1,2]{2,1,0:T(2,128)(2,1)S(1)} %bitcast.144), channel_id=1, replica_groups=mesh['sp'=8,'tp'=4] {'sp'}, dimensions={0}, use_global_device_ids=true | all-gather | bytes 36 | tf_op jit(solution)/shard_map/all_gather | solution.py:38
  36.3 9.5 %while.26 = (s32[]{:T(128)}, f32[2,128,128]{2,1,0:T(8,128)S(1)}, f32[2,2,512,128]{3,2,1,0:T(8,128)}, f32[2,2,512]{2,1,0:T(2,128)S(1)}, bf16[2,2,512,128]{3,1,2,0...) while((s32[]{:T(128)}, f32[2,128,128]{2,1,0:T(8,128)S(1)}, ...), condition=%wide.region_3.4_spmd.clone, body=%wide.region_0.3_spmd.clone.sunk | while | flops 507643936 | bytes 5702008 | solution.py:132
  45.8 2.4 copy.57
  48.2 2.1 reshape.175
  50.5 33.7 %all-gather = bf16[16,128,128]{2,1,0:T(8,128)(2,1)S(1)} all-gather(bf16[2,128,128]{2,1,0:T(8,128)(2,1)S(1)} %convert_element_type.103), channel_id=2, replica_groups=mesh['sp'=8,'tp'=4] {'sp'}, dimensions={0}, use_global_device_ids=true | all-gather | bytes 589824 | tf_op jit(solution)/shard_map/all_gather | solution.py:38
  85.9 11.2 %all_to_all.16 = bf16[4,256,256]{1,2,0:T(8,128)(2,1)S(1)} all-to-all(bf16[4,256,256]{1,2,0:T(8,128)(2,1)S(1)} %copy.62), channel_id=1, replica_groups=mesh['sp'=8,'tp'=4] {'tp'}, dimensions={0} | all-to-all | bytes 1048576 | tf_op jit(solution)/shard_map/all_to_all | solution.py:148
  104.2 36.8 %collective-permute-done = bf16[1408,256]{1,0:T(8,128)(2,1)S(1)} collective-permute-done((bf16[1408,256]{1,0:T(8,128)(2,1)S(1)}, bf16[1408,256]{1,0:T(8,128)(2,1)S(1)}, u32[]{:S(2)}, u32[]{:S(2)}) %collective-permute-start) | collective-permute-done | bytes 720928 | tf_op jit(solution)/shard_map/ppermute | solution.py:23
  141.0 33.8 %collective-permute-done.1 = bf16[1408,256]{1,0:T(8,128)(2,1)S(1)} collective-permute-done((bf16[1408,256]{1,0:T(8,128)(2,1)S(1)}, bf16[1408,256]{1,0:T(8,128)(2,1)S(1)}, u32[]{:S(2)}, u32[]{:S(2)}) %collective-permute-start.1) | collective-permute-done | bytes 720928 | tf_op jit(solution)/shard_map/ppermute | solution.py:23
  174.8 20.2 %collective-permute-done.2 = bf16[1408,256]{1,0:T(8,128)(2,1)S(1)} collective-permute-done((bf16[1408,256]{1,0:T(8,128)(2,1)S(1)}, bf16[1408,256]{1,0:T(8,128)(2,1)S(1)}, u32[]{:S(2)}, u32[]{:S(2)}) %collective-permute-start.2) | collective-permute-done | bytes 720928 | tf_op jit(solution)/shard_map/ppermute | solution.py:23
  195.9 19.3 %collective-permute-done.3 = bf16[1408,256]{1,0:T(8,128)(2,1)S(1)} collective-permute-done((bf16[1408,256]{1,0:T(8,128)(2,1)S(1)}, bf16[1408,256]{1,0:T(8,128)(2,1)S(1)}, u32[]{:S(2)}, u32[]{:S(2)}) %collective-permute-start.3) | collective-permute-done | bytes 720928 | tf_op jit(solution)/shard_map/ppermute | solution.py:23
  216.0 33.3 %collective-permute-done.4 = bf16[1408,256]{1,0:T(8,128)(2,1)S(1)} collective-permute-done((bf16[1408,256]{1,0:T(8,128)(2,1)S(1)}, bf16[1408,256]{1,0:T(8,128)(2,1)S(1)}, u32[]{:S(2)}, u32[]{:S(2)}) %collective-permute-start.4) | collective-permute-done | bytes 720928 | tf_op jit(solution)/shard_map/ppermute | solution.py:23
  250.2 23.2 %collective-permute-done.5 = bf16[1408,256]{1,0:T(8,128)(2,1)} collective-permute-done((bf16[1408,256]{1,0:T(8,128)(2,1)S(1)}, bf16[1408,256]{1,0:T(8,128)(2,1)}, u32[]{:S(2)}, u32[]{:S(2)}) %collective-permute-start.5) | collective-permute-done | bytes 720928 | tf_op jit(solution)/shard_map/ppermute | solution.py:23
  273.3 36.0 %collective-permute-done.6 = bf16[1408,256]{1,0:T(8,128)(2,1)} collective-permute-done((bf16[1408,256]{1,0:T(8,128)(2,1)}, bf16[1408,256]{1,0:T(8,128)(2,1)}, u32[]{:S(2)}, u32[]{:S(2)}) %collective-permute-start.6) | collective-permute-done | bytes 720928 | tf_op jit(solution)/shard_map/ppermute | solution.py:23
  309.4 2.1 constant_dynamic-update-slice_fusion.15
  311.5 2.1 constant_dynamic-update-slice_fusion.14
  313.6 2.1 constant_dynamic-update-slice_fusion.13
  315.7 2.2 constant_dynamic-update-slice_fusion.12
  321.7 2.1 constant_dynamic-update-slice_fusion.7
  323.8 2.1 constant_dynamic-update-slice_fusion.6
  331.7 11.7 %fusion.59 = f32[1024,1408]{1,0:T(8,128)} fusion(bf16[1024,2048]{1,0:T(8,128)(2,1)} %all-gather.9.cloned.1.call-done, bf16[2048,1408]{1,0:T(8,128)(2,1)} %all-gather.11.cloned.1.call-done), kind=kOutput, calls=%fused_computation.117 | convolution fusion | flops 5905580032 | bytes 15728640 | tf_op jit(solution)/shard_map/dot_general | solution.py:167
  343.4 20.6 %fusion.19 = bf16[1024,2048]{1,0:T(8,128)(2,1)} fusion(bf16[1408,4096]{1,0:T(8,128)(2,1)} %constant_dynamic-update-slice_fusion, s32[]{:T(128)S(6)} %select_n.25, f32[1024,1408]{1,0:T(8,128)} %fusion.59, bf16[1024,2048]{1,0:T(8,128)(2,1)} %all-gather.9.cloned.1.call-done, bf16[2048,1408]{1,0:T(8,128)(2,1)} %all-gather.13.cloned.1.call-done), kind=kOutput, calls=%fused_computation.40 | convolution fusion | flops 11821907968 | bytes 25690116 | tf_op jit(solution)/shard_map/dot_general | solution.py:178
  364.0 48.6 %reduce-scatter.2.cloned.1.call-done = bf16[256,2048]{1,0:T(8,128)(2,1)} async-done(((bf16[1024,2048]{1,0:T(8,128)(2,1)}), bf16[256,2048]{1,0:T(8,128)(2,1)}) %reduce-scatter.2.cloned.1.call-update) | async-done | bytes 1048592 | tf_op jit(solution)/shard_map/reduce_scatter | solution.py:177
  414.2 2.6 fusion.39
  (133 shorter events, 37.1 us)
Async XLA Ops:
  6.5 6.1 %copy-start.9 = (bf16[1024,256]{1,0:T(8,128)(2,1)S(1)}, bf16[1024,256]{1,0:T(8,128)(2,1)}, u32[]{:S(2)}) copy-start(bf16[1024,256]{1,0:T(8,128)(2,1)} %param.18) | copy-start | bytes 1572868
  6.5 6.2 %copy-start.12 = (f32[1024,2]{0,1:T(2,128)S(1)}, f32[1024,2]{0,1:T(2,128)}, u32[]{:S(2)}) copy-start(f32[1024,2]{0,1:T(2,128)} %param.22) | copy-start | bytes 24580
  6.5 90.6 %all-gather.7.cloned.1.call-start = ((), (), s32[]{:S(2)}) async-start(), calls=%async_computation.2 | async-start | bytes 5242880 | tf_op jit(solution)/shard_map/all_gather | solution.py:152
  7.3 324.5 %all-gather.11.cloned.1.call-start = ((), (), s32[]{:S(2)}) async-start(), calls=%async_computation.4 | async-start | bytes 6488064 | tf_op jit(solution)/shard_map/all_gather | solution.py:169
  8.0 323.7 %all-gather.9.cloned.1.call-start = ((), (), s32[]{:S(2)}) async-start(), calls=%async_computation.3 | async-start | bytes 5242880 | tf_op jit(solution)/shard_map/all_gather | solution.py:165
  45.8 38.4 %copy-start.10 = (bf16[1024,256]{1,0:T(8,128)(2,1)S(1)}, bf16[1024,256]{1,0:T(8,128)(2,1)}, u32[]{:S(2)}) copy-start(bf16[1024,256]{1,0:T(8,128)(2,1)} %param.18) | copy-start | bytes 1572868
  45.8 39.3 %copy-start.1 = (f32[1024,256]{0,1:T(8,128)S(1)}, f32[1024,256]{0,1:T(8,128)}, u32[]{:S(2)}) copy-start(f32[1024,256]{0,1:T(8,128)} %copy.53) | copy-start | bytes 3145732
  45.8 39.3 %copy-start.16 = (f32[2,128]{1,0:T(2,128)S(1)}, f32[2,128]{1,0:T(2,128)}, u32[]{:S(2)}) copy-start(f32[2,128]{1,0:T(2,128)} %param.23) | copy-start | bytes 3076
  97.2 3.5 copy-start
  101.2 1.5 copy-start.14
  101.2 2.9 copy-start.2
  104.0 239.4 %all-gather.13.cloned.1.call-start = ((), (), s32[]{:S(2)}) async-start(), calls=%async_computation.5 | async-start | bytes 6488064 | tf_op jit(solution)/shard_map/all_gather | solution.py:173
  104.1 36.9 %collective-permute-start = (bf16[1408,256]{1,0:T(8,128)(2,1)S(1)}, bf16[1408,256]{1,0:T(8,128)(2,1)S(1)}, u32[]{:S(2)}, u32[]{:S(2)}) collective-permute-start(bf16[1408,256]{1,0:T(8,128)(2,1)S(1)} %copy-done.2), channel_id=1, source_target_pairs={{0,4},{4,8},{8,12},{12,16},{16,20},{20,24},{24,28},{28,0},{1,5},{5... | collective-permute-start | bytes 2162696 | tf_op jit(solution)/shard_map/ppermute | solution.py:23
  141.0 33.8 %collective-permute-start.1 = (bf16[1408,256]{1,0:T(8,128)(2,1)S(1)}, bf16[1408,256]{1,0:T(8,128)(2,1)S(1)}, u32[]{:S(2)}, u32[]{:S(2)}) collective-permute-start(bf16[1408,256]{1,0:T(8,128)(2,1)S(1)} %collective-permute-done), channel_id=1, source_target_pairs={{0,4},{4,8},{8,12},{12,16},{16,20},{20,24},{24,28},{28,0},{1,5},{5... | collective-permute-start | bytes 2162696 | tf_op jit(solution)/shard_map/ppermute | solution.py:23
  141.0 271.6 %reduce-scatter.2.cloned.1.call-start = ((), (), s32[]{:S(2)}) async-start(), calls=%async_computation.6 | async-start | bytes 5242880 | tf_op jit(solution)/shard_map/reduce_scatter | solution.py:177
  174.8 20.2 %collective-permute-start.2 = (bf16[1408,256]{1,0:T(8,128)(2,1)S(1)}, bf16[1408,256]{1,0:T(8,128)(2,1)S(1)}, u32[]{:S(2)}, u32[]{:S(2)}) collective-permute-start(bf16[1408,256]{1,0:T(8,128)(2,1)S(1)} %collective-permute-done.1), channel_id=1, source_target_pairs={{0,4},{4,8},{8,12},{12,16},{16,20},{20,24},{24,28},{28,0},{1,5},{5... | collective-permute-start | bytes 2162696 | tf_op jit(solution)/shard_map/ppermute | solution.py:23
  195.8 19.3 %collective-permute-start.3 = (bf16[1408,256]{1,0:T(8,128)(2,1)S(1)}, bf16[1408,256]{1,0:T(8,128)(2,1)S(1)}, u32[]{:S(2)}, u32[]{:S(2)}) collective-permute-start(bf16[1408,256]{1,0:T(8,128)(2,1)S(1)} %collective-permute-done.2), channel_id=1, source_target_pairs={{0,4},{4,8},{8,12},{12,16},{16,20},{20,24},{24,28},{28,0},{1,5},{5... | collective-permute-start | bytes 2162696 | tf_op jit(solution)/shard_map/ppermute | solution.py:23
  216.0 33.3 %collective-permute-start.4 = (bf16[1408,256]{1,0:T(8,128)(2,1)S(1)}, bf16[1408,256]{1,0:T(8,128)(2,1)S(1)}, u32[]{:S(2)}, u32[]{:S(2)}) collective-permute-start(bf16[1408,256]{1,0:T(8,128)(2,1)S(1)} %collective-permute-done.3), channel_id=1, source_target_pairs={{0,4},{4,8},{8,12},{12,16},{16,20},{20,24},{24,28},{28,0},{1,5},{5... | collective-permute-start | bytes 2162696 | tf_op jit(solution)/shard_map/ppermute | solution.py:23
  250.2 23.2 %collective-permute-start.5 = (bf16[1408,256]{1,0:T(8,128)(2,1)S(1)}, bf16[1408,256]{1,0:T(8,128)(2,1)}, u32[]{:S(2)}, u32[]{:S(2)}) collective-permute-start(bf16[1408,256]{1,0:T(8,128)(2,1)S(1)} %collective-permute-done.4), channel_id=1, source_target_pairs={{0,4},{4,8},{8,12},{12,16},{16,20},{20,24},{24,28},{28,0},{1,5},{5... | collective-permute-start | bytes 2162696 | tf_op jit(solution)/shard_map/ppermute | solution.py:23
  273.3 36.0 %collective-permute-start.6 = (bf16[1408,256]{1,0:T(8,128)(2,1)}, bf16[1408,256]{1,0:T(8,128)(2,1)}, u32[]{:S(2)}, u32[]{:S(2)}) collective-permute-start(bf16[1408,256]{1,0:T(8,128)(2,1)} %collective-permute-done.5), channel_id=1, source_target_pairs={{0,4},{4,8},{8,12},{12,16},{16,20},{20,24},{24,28},{28,0},{1,5},{5... | collective-permute-start | bytes 2162696 | tf_op jit(solution)/shard_map/ppermute | solution.py:23
  273.3 44.6 %copy-start.4 = (bf16[1408,256]{1,0:T(8,128)(2,1)S(1)}, bf16[1408,256]{1,0:T(8,128)(2,1)}, u32[]{:S(2)}) copy-start(bf16[1408,256]{1,0:T(8,128)(2,1)} %copy-done.3) | copy-start | bytes 2162692
  313.6 12.3 %copy-start.8 = (bf16[1408,256]{1,0:T(8,128)(2,1)S(1)}, bf16[1408,256]{1,0:T(8,128)(2,1)}, u32[]{:S(2)}) copy-start(bf16[1408,256]{1,0:T(8,128)(2,1)} %copy-done.7) | copy-start | bytes 2162692
  315.7 11.2 %copy-start.6 = (bf16[1408,256]{1,0:T(8,128)(2,1)S(1)}, bf16[1408,256]{1,0:T(8,128)(2,1)}, u32[]{:S(2)}) copy-start(bf16[1408,256]{1,0:T(8,128)(2,1)} %copy-done.5) | copy-start | bytes 2162692
  343.4 70.8 %copy-start.15 = (f32[2048]{0:T(1024)S(1)}, f32[2048]{0:T(1024)}, u32[]{:S(2)}) copy-start(f32[2048]{0:T(1024)} %param.31) | copy-start | bytes 24580
  (5 other events, 5.2 us)
Sparse Core Ops, SparseCore 0:
  8.9 37.1 all-gather.6
  48.3 109.3 all-gather.10
  159.2 48.7 all-gather.8
  210.1 125.8 all-gather.12
  364.1 48.4 reduce-scatter.1
